TPU v7x, 32 devices: a whole 2x2x4 slice. The times are simulated.
32 devices in a mesh: grp: 2 (over y), sp: 4 (over z), tp: 4 (over x, core).
Axes of the slice: x: 2, y: 2, z: 4, core: 2. Of those that a mesh axis runs over, the one named last changes fastest.
Arguments:
- tokens: bfloat16 [1024, 2048], P(('grp', 'sp')), parts along dimension 0, may hold values from -8 to 8
- norm_gain: float32 [2048], replicated, may hold values from 0.1 to 1.9
- w_query: bfloat16 [2048, 1024], P(None, 'tp'), may hold values from -0.125 to 0.125
- w_key: bfloat16 [2048, 1024], P(None, 'tp'), may hold values from -0.125 to 0.125
- w_value: bfloat16 [2048, 1024], P(None, 'tp'), may hold values from -0.125 to 0.125
- w_out: bfloat16 [1024, 2048], P('tp'), may hold values from -0.1875 to 0.1875
- key_rate: bfloat16 [16, 1024], P('tp', ('grp', 'sp')), parts along dimension 1, may hold values from -16 to 1
Outputs:
- layer_out: bfloat16 [1024, 2048], P(('grp', 'sp')), parts along dimension 0
There are 2 independent parts, one for each index of `grp`. A program takes and returns all parts, laid end to end along the dimension named above; an argument that names none is the same for every part. Nothing has to cross between parts.
All inputs are finite; a program needn't handle non-finite values.
Results may differ from a plain program's by a relative error of at most 0.0075.
Values may be sent and summed in bfloat16 or wider, within the bound.
No kernel may reach another device: no remote copies, remote signals or barrier semaphores. Data moves between devices by JAX's collectives and lax.ppermute only.
A program may use at most 64 MiB of HBM per device.

v0:
```python
import jax
import jax.numpy as jnp
from jax import lax
from jax.sharding import PartitionSpec as P

HD = 64
KEY_SPAN = 128
F32 = jnp.float32
BF16 = jnp.bfloat16
HIGHEST = lax.Precision.HIGHEST
EPS = 1e-06


def break_scores(query_heads, key_heads, rate_row_values, query_pos, key_pos):
    scores = jnp.einsum(
        "qhd,khd->hqk", query_heads, key_heads, preferred_element_type=F32
    ) * HD ** (-0.5)
    scores = scores + jnp.transpose(rate_row_values).astype(F32)[:, None, :]
    causal_mask = key_pos[None, :] < query_pos[:, None]
    log_remain = jnp.where(causal_mask[None], jax.nn.log_sigmoid(-scores), 0.0)
    return (scores, causal_mask, log_remain)


def shard_summary(query_heads, key_heads, value_heads, rate_row_values, query_pos, key_pos):
    scores, causal_mask, log_remain = break_scores(
        query_heads, key_heads, rate_row_values, query_pos, key_pos
    )
    heads_here, query_count, key_count = scores.shape
    span_count = key_count // KEY_SPAN
    blocks = log_remain.reshape(heads_here, query_count, span_count, KEY_SPAN)
    span_ids = jnp.arange(KEY_SPAN, dtype=jnp.int32)
    tri_strict = (span_ids[:, None] > span_ids[None, :]).astype(F32)
    inside_sum = jnp.einsum("hqnj,js->hqns", blocks, tri_strict, precision=HIGHEST)
    block_ids = jnp.arange(span_count, dtype=jnp.int32)
    block_later = (block_ids[:, None] > block_ids[None, :]).astype(F32)
    beyond = jnp.einsum("hqn,nm->hqm", jnp.sum(blocks, axis=-1), block_later, precision=HIGHEST)
    suffix = (inside_sum + beyond[..., None]).reshape(heads_here, query_count, key_count)
    weight = jnp.where(causal_mask[None], jnp.exp(jax.nn.log_sigmoid(scores) + suffix), 0.0).astype(
        BF16
    )
    partial_value = jnp.einsum("hqk,khd->qhd", weight, value_heads, preferred_element_type=F32)
    return (partial_value.reshape(query_count, heads_here * HD), jnp.sum(log_remain, axis=-1))


def on_device(tokens, norm_gain, w_query, w_key, w_value, w_out, key_rate):
    tokens_f = tokens.astype(F32)
    normed = (
        tokens_f
        * lax.rsqrt(jnp.mean(tokens_f * tokens_f, axis=-1, keepdims=True) + EPS)
        * norm_gain
    ).astype(BF16)
    queries = jnp.dot(normed, w_query, preferred_element_type=F32).astype(BF16)
    key_rows = jnp.dot(normed, w_key, preferred_element_type=F32).astype(BF16)
    value_rows = jnp.dot(normed, w_value, preferred_element_type=F32).astype(BF16)
    head_width = w_query.shape[1]
    heads_local = head_width // HD
    row_count = tokens.shape[0]
    rate_row_values = jnp.transpose(key_rate)
    query_heads = queries.reshape(row_count, heads_local, HD)
    own_shard = lax.axis_index("sp")
    shard_total = lax.axis_size("sp")
    local_pos = jnp.arange(row_count, dtype=jnp.int32)
    shard_ids = jnp.arange(shard_total, dtype=jnp.int32)
    later_mask = (shard_ids[:, None] > shard_ids[None, :]).astype(F32)
    query_groups = [(query_heads, own_shard * row_count)]

    def summarize(key_block, value_block, rate_block, first_key):
        key_pos = first_key + local_pos
        group_heads, group_start = query_groups[0]
        group_count = group_heads.shape[0]
        group_pos = group_start + jnp.arange(group_count, dtype=jnp.int32)
        empty_pair = (
            jnp.zeros((group_count, head_width), F32),
            jnp.zeros((heads_local, group_count), F32),
        )
        partial_value, remain = lax.cond(
            first_key < group_start + group_count - 1,
            lambda: shard_summary(
                group_heads, key_block, value_block, rate_block, group_pos, key_pos
            ),
            lambda: empty_pair,
        )
        partial_list = [partial_value]
        remain_list = [remain]
        return (jnp.concatenate(partial_list, axis=0), jnp.concatenate(remain_list, axis=1))

    initial = (
        jnp.zeros((shard_total, row_count, head_width), F32),
        jnp.zeros((shard_total, heads_local, row_count), F32),
    )
    piece_keys = lax.all_gather(key_rows, "sp", axis=0, tiled=True)
    piece_values = lax.all_gather(value_rows, "sp", axis=0, tiled=True)
    piece_rates = lax.all_gather(rate_row_values, "sp", axis=0, tiled=True)
    piece_count = piece_keys.shape[0] // row_count
    key_blocks = piece_keys.reshape(piece_count, row_count, heads_local, HD)
    value_blocks = piece_values.reshape(piece_count, row_count, heads_local, HD)
    rate_blocks = piece_rates.reshape(piece_count, row_count, heads_local)

    def absorb_one(inner_pair, item_tuple):
        item_index, key_block, value_block, rate_block = item_tuple
        first_key = item_index * row_count
        shard_index = first_key // row_count
        partial_value, remain = summarize(key_block, value_block, rate_block, first_key)
        partials = lax.dynamic_update_index_in_dim(inner_pair[0], partial_value, shard_index, 0)
        remains = lax.dynamic_update_index_in_dim(inner_pair[1], remain, shard_index, 0)
        return ((partials, remains), None)

    result, _ = lax.scan(
        absorb_one,
        initial,
        (jnp.arange(piece_count, dtype=jnp.int32), key_blocks, value_blocks, rate_blocks),
    )
    partials, remains = result
    beyond = jnp.einsum("nhq,nm->mhq", remains, later_mask, precision=HIGHEST)
    factor = jnp.transpose(jnp.exp(beyond), (0, 2, 1))[..., None]
    mixed_rows = jnp.sum(partials.reshape(shard_total, row_count, heads_local, HD) * factor, axis=0)
    mixed = mixed_rows.reshape(row_count, head_width).astype(BF16)
    token_heads = lax.all_to_all(mixed, "tp", split_axis=0, concat_axis=1, tiled=True)
    whole_out = lax.all_gather(w_out, "tp", axis=0, tiled=True)
    own_rows = jnp.dot(token_heads, whole_out, preferred_element_type=F32).astype(BF16)
    return lax.all_gather(own_rows, "tp", axis=0, tiled=True)


def solution(mesh):
    return jax.shard_map(
        on_device,
        mesh=mesh,
        in_specs=(
            P(("grp", "sp"), None),
            P(),
            P(None, "tp"),
            P(None, "tp"),
            P(None, "tp"),
            P("tp", None),
            P("tp", ("grp", "sp")),
        ),
        out_specs=P(("grp", "sp"), None),
        check_vma=False,
    )
```

profile of v0, /device:TPU:25, one launch (start us, length us, event | category | flops | bytes accessed | tf_op | source)
XLA Modules:
  0.0 93.3 jit_solution(17264272396755167459)
XLA Ops:
  6.5 0.0 copy-start
  6.5 0.0 copy-start.1
  6.5 0.0 copy-start.3
  6.5 0.0 all-gather.2.cloned.1.call-start
  6.5 0.7 all-gather.2.cloned.1.call-update
  7.3 1.2 %fusion.25 = f32[128]{0:T(128)S(1)} fusion(bf16[128,2048]{1,0:T(8,128)(2,1)} %param.11), kind=kLoop, calls=%fused_computation.40 | loop fusion | flops 786304 | bytes 524800 | tf_op jit(solution)/shard_map/reduce_sum | solution.py:49
  8.5 0.0 copy-done
  8.5 1.4 %convolution_convert_fusion.3 = bf16[128,256]{1,0:T(8,128)(2,1)S(1)} fusion(bf16[2048,256]{1,0:T(8,128)(2,1)S(1)} %copy-done, bf16[128,2048]{1,0:T(8,128)(2,1)} %param.11, f32[2048]{0:T(1024)} %param.12, f32[128]{0:T(128)S(1)} %add_rsqrt_fusion), kind=kOutput, calls=%fused_computation.37 | convolution fusion | flops 135299072 | bytes 1647104 | tf_op jit(solution)/shard_map/dot_general | solution.py:53
  9.9 0.0 copy-start.2
  9.9 11.0 %all_gather.15 = bf16[512,256]{1,0:T(8,128)(2,1)S(1)} all-gather(bf16[128,256]{1,0:T(8,128)(2,1)S(1)} %convolution_convert_fusion.3), channel_id=1, replica_groups=mesh['grp'=2,'sp'=4,'tp'=4] {'sp'}, dimensions={0}, use_global_device_ids=true | all-gather | bytes 327680 | tf_op jit(solution)/shard_map/all_gather | solution.py:91
  20.9 0.2 reshape.91
  21.2 0.3 copy.39
  21.5 0.0 copy-done.1
  21.5 0.0 copy-done.3
  21.5 1.6 %convolution_convert_fusion.1 = bf16[128,256]{1,0:T(8,128)(2,1)S(1)} fusion(bf16[2048,256]{1,0:T(8,128)(2,1)} %param.15, bf16[128,2048]{1,0:T(8,128)(2,1)S(1)} %copy-done.1, f32[2048]{0:T(1024)S(1)} %copy-done.3, f32[128]{0:T(128)S(1)} %add_rsqrt_fusion), kind=kOutput, calls=%fused_computation.35 | convolution fusion | flops 135299072 | bytes 1647104 | tf_op jit(solution)/shard_map/dot_general | solution.py:54
  23.1 12.0 %all_gather.17 = bf16[512,256]{1,0:T(8,128)(2,1)S(1)} all-gather(bf16[128,256]{1,0:T(8,128)(2,1)S(1)} %convolution_convert_fusion.1), channel_id=1, replica_groups=mesh['grp'=2,'sp'=4,'tp'=4] {'sp'}, dimensions={0}, use_global_device_ids=true | all-gather | bytes 327680 | tf_op jit(solution)/shard_map/all_gather | solution.py:92
  35.1 0.2 reshape.92
  35.3 0.3 copy.40
  35.6 1.6 %convolution_convert_fusion.2 = bf16[128,256]{1,0:T(8,128)(2,1)S(1)} fusion(bf16[2048,256]{1,0:T(8,128)(2,1)} %param.13, bf16[128,2048]{1,0:T(8,128)(2,1)S(1)} %copy-done.1, f32[2048]{0:T(1024)S(1)} %copy-done.3, f32[128]{0:T(128)S(1)} %add_rsqrt_fusion), kind=kOutput, calls=%fused_computation.36 | convolution fusion | flops 135299072 | bytes 1647104 | tf_op jit(solution)/shard_map/dot_general | solution.py:52
  37.2 0.1 copy.37
  37.3 0.0 copy-done.2
  37.3 5.6 %all_gather.16 = bf16[512,4]{0,1:T(4,128)(2,1)S(1)} all-gather(bf16[128,4]{0,1:T(4,128)(2,1)S(1)} %bitcast.58), channel_id=1, replica_groups=mesh['grp'=2,'sp'=4,'tp'=4] {'sp'}, dimensions={0}, use_global_device_ids=true | all-gather | bytes 5120 | tf_op jit(solution)/shard_map/all_gather | solution.py:93
  43.0 18.4 %while.16 = (s32[]{:T(128)}, f32[4,128,256]{1,2,0:T(8,128)S(1)}, f32[4,4,128]{2,0,1:T(4,128)S(1)}, s32[4]{0:T(128)S(1)}, s32[]{:T(128)}, /*index=5*/s32[]{:T(128...) while((s32[]{:T(128)}, f32[4,128,256]{1,2,0:T(8,128)S(1)}, ...), condition=%wide.region_5.6_spmd.clone, body=%wide.region_1.5_spmd.clone.sunk | while | flops 119505664 | bytes 1446895 | solution.py:108
  43.0 0.6 dynamic_slice.50
  44.3 2.6 %conditional.3 = (f32[1,128,256]{1,2,0:T(8,128)S(1)}, f32[1,4,128]{2,1,0:T(4,128)}) conditional(s32[]{:T(128)} %convert_element_type.82, () %tuple.61, (s32[]{:T(128)}, s32[128]{0:T(128)S(1)}, s32[]{:T(128)}, s32[128]{0:T(128)S(1)}, bf16[4,128,4,64]{1,3,2,0:T(8,128)(2,1)S(1)}, /*index=5*/s32[]{:T(128)}, bf16[128,4,64]{0,2,1:T(8,128)(2,1)S(1)}, ...), branch_computations={%region_2.2_spmd, %region_3.4_spmd} | conditional | flops 119505664 | bytes 1179684 | solution.py:76
  44.3 0.1 broadcast_compare_fusion
  44.4 1.0 %fusion.11 = (f32[4,128]{1,0:T(4,128)}, f32[4,128,128]{1,2,0:T(8,128)S(1)}) fusion(pred[128,128]{0,1:T(8,128)(4,1)S(1)} %broadcast_compare_fusion, f32[4,128]{1,0:T(4,128)S(1)} %convert_bitcast_fusion, bf16[128,4,64]{0,2,1:T(8,128)(2,1)S(1)} %get-tuple-element.246, bf16[4,128,4,64]{1,3,2,0:T(8,128)(2,1)S(1)} %get-tuple-element.244, s32[]{:T(128)} %get-tuple-element.245), kind=kOutput, calls=%fused_computation.14 | convolution fusion | flops 9108992 | bytes 413700 | tf_op jit(solution)/shard_map/while/body/eval_jaxpr/cond/branch_1_fun/qhd,khd->hqk/dot_general | solution.py:15
  45.4 0.7 broadcast_multiply_fusion
  46.1 0.6 fusion.7
  46.7 0.2 fusion.14
  46.9 0.7 dynamic_update_slice.22
  47.6 0.6 dynamic_slice.50
  48.9 2.6 %conditional.3 = (f32[1,128,256]{1,2,0:T(8,128)S(1)}, f32[1,4,128]{2,1,0:T(4,128)}) conditional(s32[]{:T(128)} %convert_element_type.82, () %tuple.61, (s32[]{:T(128)}, s32[128]{0:T(128)S(1)}, s32[]{:T(128)}, s32[128]{0:T(128)S(1)}, bf16[4,128,4,64]{1,3,2,0:T(8,128)(2,1)S(1)}, /*index=5*/s32[]{:T(128)}, bf16[128,4,64]{0,2,1:T(8,128)(2,1)S(1)}, ...), branch_computations={%region_2.2_spmd, %region_3.4_spmd} | conditional | flops 119505664 | bytes 1179684 | solution.py:76
  48.9 0.1 broadcast_compare_fusion
  49.0 1.0 %fusion.11 = (f32[4,128]{1,0:T(4,128)}, f32[4,128,128]{1,2,0:T(8,128)S(1)}) fusion(pred[128,128]{0,1:T(8,128)(4,1)S(1)} %broadcast_compare_fusion, f32[4,128]{1,0:T(4,128)S(1)} %convert_bitcast_fusion, bf16[128,4,64]{0,2,1:T(8,128)(2,1)S(1)} %get-tuple-element.246, bf16[4,128,4,64]{1,3,2,0:T(8,128)(2,1)S(1)} %get-tuple-element.244, s32[]{:T(128)} %get-tuple-element.245), kind=kOutput, calls=%fused_computation.14 | convolution fusion | flops 9108992 | bytes 413700 | tf_op jit(solution)/shard_map/while/body/eval_jaxpr/cond/branch_1_fun/qhd,khd->hqk/dot_general | solution.py:15
  50.0 0.7 broadcast_multiply_fusion
  50.7 0.6 fusion.7
  51.3 0.2 fusion.14
  51.5 0.7 dynamic_update_slice.22
  52.2 0.6 dynamic_slice.50
  53.5 2.6 %conditional.3 = (f32[1,128,256]{1,2,0:T(8,128)S(1)}, f32[1,4,128]{2,1,0:T(4,128)}) conditional(s32[]{:T(128)} %convert_element_type.82, () %tuple.61, (s32[]{:T(128)}, s32[128]{0:T(128)S(1)}, s32[]{:T(128)}, s32[128]{0:T(128)S(1)}, bf16[4,128,4,64]{1,3,2,0:T(8,128)(2,1)S(1)}, /*index=5*/s32[]{:T(128)}, bf16[128,4,64]{0,2,1:T(8,128)(2,1)S(1)}, ...), branch_computations={%region_2.2_spmd, %region_3.4_spmd} | conditional | flops 119505664 | bytes 1179684 | solution.py:76
  53.5 0.1 broadcast_compare_fusion
  53.6 1.0 %fusion.11 = (f32[4,128]{1,0:T(4,128)}, f32[4,128,128]{1,2,0:T(8,128)S(1)}) fusion(pred[128,128]{0,1:T(8,128)(4,1)S(1)} %broadcast_compare_fusion, f32[4,128]{1,0:T(4,128)S(1)} %convert_bitcast_fusion, bf16[128,4,64]{0,2,1:T(8,128)(2,1)S(1)} %get-tuple-element.246, bf16[4,128,4,64]{1,3,2,0:T(8,128)(2,1)S(1)} %get-tuple-element.244, s32[]{:T(128)} %get-tuple-element.245), kind=kOutput, calls=%fused_computation.14 | convolution fusion | flops 9108992 | bytes 413700 | tf_op jit(solution)/shard_map/while/body/eval_jaxpr/cond/branch_1_fun/qhd,khd->hqk/dot_general | solution.py:15
  54.6 0.7 broadcast_multiply_fusion
  55.3 0.6 fusion.7
  55.9 0.2 fusion.14
  56.1 0.7 dynamic_update_slice.22
  56.8 0.6 dynamic_slice.50
  58.1 2.6 %conditional.3 = (f32[1,128,256]{1,2,0:T(8,128)S(1)}, f32[1,4,128]{2,1,0:T(4,128)}) conditional(s32[]{:T(128)} %convert_element_type.82, () %tuple.61, (s32[]{:T(128)}, s32[128]{0:T(128)S(1)}, s32[]{:T(128)}, s32[128]{0:T(128)S(1)}, bf16[4,128,4,64]{1,3,2,0:T(8,128)(2,1)S(1)}, /*index=5*/s32[]{:T(128)}, bf16[128,4,64]{0,2,1:T(8,128)(2,1)S(1)}, ...), branch_computations={%region_2.2_spmd, %region_3.4_spmd} | conditional | flops 119505664 | bytes 1179684 | solution.py:76
  58.1 0.1 broadcast_compare_fusion
  58.2 1.0 %fusion.11 = (f32[4,128]{1,0:T(4,128)}, f32[4,128,128]{1,2,0:T(8,128)S(1)}) fusion(pred[128,128]{0,1:T(8,128)(4,1)S(1)} %broadcast_compare_fusion, f32[4,128]{1,0:T(4,128)S(1)} %convert_bitcast_fusion, bf16[128,4,64]{0,2,1:T(8,128)(2,1)S(1)} %get-tuple-element.246, bf16[4,128,4,64]{1,3,2,0:T(8,128)(2,1)S(1)} %get-tuple-element.244, s32[]{:T(128)} %get-tuple-element.245), kind=kOutput, calls=%fused_computation.14 | convolution fusion | flops 9108992 | bytes 413700 | tf_op jit(solution)/shard_map/while/body/eval_jaxpr/cond/branch_1_fun/qhd,khd->hqk/dot_general | solution.py:15
  59.2 0.7 broadcast_multiply_fusion
  59.9 0.6 fusion.7
  60.5 0.2 fusion.14
  60.7 0.7 dynamic_update_slice.22
  61.4 0.1 fusion.24
  61.6 0.1 copy.43
  61.7 13.7 %all_to_all.16 = bf16[4,32,256]{2,1,0:T(8,128)(2,1)S(1)} all-to-all(bf16[4,32,256]{2,1,0:T(8,128)(2,1)S(1)} %bitcast.54), channel_id=1, replica_groups=mesh['grp'=2,'sp'=4,'tp'=4] {'tp'}, dimensions={0} | all-to-all | bytes 131072 | tf_op jit(solution)/shard_map/all_to_all | solution.py:118
  75.4 0.0 all-gather.2.cloned.1.call-done
  75.4 3.0 %convolution_convert_fusion = bf16[32,2048]{1,0:T(8,128)(2,1)S(1)} fusion(bf16[32,1024]{1,0:T(8,128)(2,1)S(1)} %bitcast.53, bf16[1024,2048]{1,0:T(8,128)(2,1)} %all-gather.2.cloned.1.call-done), kind=kOutput, calls=%fused_computation.32 | convolution fusion | flops 134283264 | bytes 4390912 | tf_op jit(solution)/shard_map/dot_general | solution.py:120
  78.4 7.3 %all_gather.19 = bf16[128,2048]{1,0:T(8,128)(2,1)S(1)} all-gather(bf16[32,2048]{1,0:T(8,128)(2,1)S(1)} %convolution_convert_fusion), channel_id=1, replica_groups=mesh['grp'=2,'sp'=4,'tp'=4] {'tp'}, dimensions={0}, use_global_device_ids=true | all-gather | bytes 655360 | tf_op jit(solution)/shard_map/all_gather | solution.py:121
  85.7 0.8 copy.73
  (23 shorter events, 0.3 us)
Async XLA Ops:
  6.5 2.0 %copy-start = (bf16[2048,256]{1,0:T(8,128)(2,1)S(1)}, bf16[2048,256]{1,0:T(8,128)(2,1)}, u32[]{:S(2)}) copy-start(bf16[2048,256]{1,0:T(8,128)(2,1)} %param.14) | copy-start | bytes 3145732
  6.5 14.9 %copy-start.1 = (bf16[128,2048]{1,0:T(8,128)(2,1)S(1)}, bf16[128,2048]{1,0:T(8,128)(2,1)}, u32[]{:S(2)}) copy-start(bf16[128,2048]{1,0:T(8,128)(2,1)} %param.11) | copy-start | bytes 1572868
  6.5 14.9 %copy-start.3 = (f32[2048]{0:T(1024)S(1)}, f32[2048]{0:T(1024)}, u32[]{:S(2)}) copy-start(f32[2048]{0:T(1024)} %param.12) | copy-start | bytes 24580
  6.5 68.8 %all-gather.2.cloned.1.call-start = ((), (), s32[]{:S(2)}) async-start(), calls=%async_computation.1 | async-start | bytes 5242880 | tf_op jit(solution)/shard_map/all_gather | solution.py:119
  9.9 27.4 %copy-start.2 = (bf16[4,128]{1,0:T(4,128)(2,1)S(1)}, bf16[4,128]{1,0:T(4,128)(2,1)}, u32[]{:S(2)}) copy-start(bf16[4,128]{1,0:T(4,128)(2,1)} %param.17) | copy-start | bytes 3076
Sparse Core Ops, SparseCore 0:
  8.9 35.8 all-gather.1
where the time goes:
time: 93.8 us; the launch traced here: 93.3 us
  blocking collectives  49.5 us (53%)
  matrix products  14.6 us (16%)
  between operations  13.5 us (14%)
  local copies, waits for them, and re-layouts  7.46 us (8%)
  other arithmetic  4.42 us (5%)
  loops' own time  3.02 us (3%)
    all_to_all x1, blocking collectives, on_device(): lax.all_to_all(mixed, 'tp', split_axis=0, concat_axis=1, tiled=True)  13.7 us
    all_gather x1, blocking collectives, on_device(): piece_values = lax.all_gather(value_rows, 'sp', axis=0, tiled=True)  12 us
    all_gather x1, blocking collectives, on_device(): piece_keys = lax.all_gather(key_rows, 'sp', axis=0, tiled=True)  11 us
    all_gather x1, blocking collectives, on_device(): return lax.all_gather(own_rows, 'tp', axis=0, tiled=True)  7.28 us
    all_gather x1, blocking collectives, on_device(): piece_rates = lax.all_gather(rate_row_values, 'sp', axis=0, tiled=True)  5.6 us
    dot_general x4, matrix products, break_scores(): jnp.einsum('qhd,khd->hqk', query_heads, key_heads, preferred_element_type...  3.93 us
    dot_general x1, matrix products, on_device(): jnp.dot(token_heads, whole_out, preferred_element_type=F32).astype(BF16)  3.01 us
    dynamic_update_slice x4, local copies, waits for them, and re-layouts, absorb_one(): lax.dynamic_update_index_in_dim(inner_pair[1], remain, shard_index, 0)  2.88 us
  transfers between devices with their start and end apart: 1, of which 0 were waited for; matrix products, arithmetic and copies ran while one was open for 24% of the time, Pallas kernels for 0%

commit v1 on v0

--- a/solution.py
+++ b/solution.py
@@ -90,7 +90,14 @@
     )
     piece_keys = lax.all_gather(key_rows, "sp", axis=0, tiled=True)
     piece_values = lax.all_gather(value_rows, "sp", axis=0, tiled=True)
-    piece_rates = lax.all_gather(rate_row_values, "sp", axis=0, tiled=True)
+    size = lax.axis_size("sp")
+    right = [(i, (i + 1) % size) for i in range(size)]
+    parts = [rate_row_values]
+    for far in range(1, size):
+        parts = [lax.ppermute(parts[0], "sp", right), *parts]
+    result_2 = jnp.concatenate(parts, axis=0)
+    shift = (lax.axis_index("sp") + 1) * parts[-1].shape[0]
+    piece_rates = jnp.roll(result_2, shift, axis=0)
     piece_count = piece_keys.shape[0] // row_count
     key_blocks = piece_keys.reshape(piece_count, row_count, heads_local, HD)
     value_blocks = piece_values.reshape(piece_count, row_count, heads_local, HD)

time: 93.8 us -> 89.4 us (0.953)
  blocking collectives: 49.5 us -> 42.9 us
  waiting for transfers between devices: 0.71 us -> 2.35 us
  starting transfers between devices: 0.01 us -> 1.56 us
  matrix products: 14.6 us -> 13.6 us
    all_gather x1 -> x0, blocking collectives: 5.6 us -> none  [on_device(): piece_rates = lax.all_gather(rate_row_values, 'sp', axis=0, tiled=True)]
    ppermute x0 -> x3, waiting for transfers between devices: none -> 1.67 us  [on_device(): parts = [lax.ppermute(parts[0], 'sp', right), *parts]]
    ppermute x0 -> x3, starting transfers between devices: none -> 1.53 us  [on_device(): parts = [lax.ppermute(parts[0], 'sp', right), *parts]]
    all_to_all x1, blocking collectives: 13.7 us -> 12.2 us  [on_device(): lax.all_to_all(mixed, 'tp', split_axis=0, concat_axis=1, tiled=True)]
    dot_general x1, matrix products: 1.58 us -> 0.37 us  [on_device(): queries = jnp.dot(normed, w_query, preferred_element_type=F32).astype(BF16)]
  transfers between devices with their start and end apart: 1 -> 4, of which waited for: 0 -> 1; matrix products, arithmetic and copies ran while one was open for 24% -> 24% of each run, Pallas kernels for 0% -> 0%
where the time goes in v1:
time: 89.4 us; the launch traced here: 88.9 us
  blocking collectives  42.9 us (48%)
  matrix products  13.6 us (15%)
  between operations  13.6 us (15%)
  local copies, waits for them, and re-layouts  7.51 us (8%)
  other arithmetic  4.41 us (5%)
  loops' own time  3.02 us (3%)
  waiting for transfers between devices  2.35 us (3%)
  starting transfers between devices  1.56 us (2%)
    all_gather x1, blocking collectives, on_device(): piece_values = lax.all_gather(value_rows, 'sp', axis=0, tiled=True)  12.3 us
    all_to_all x1, blocking collectives, on_device(): lax.all_to_all(mixed, 'tp', split_axis=0, concat_axis=1, tiled=True)  12.2 us
    all_gather x1, blocking collectives, on_device(): piece_keys = lax.all_gather(key_rows, 'sp', axis=0, tiled=True)  11.1 us
    all_gather x1, blocking collectives, on_device(): return lax.all_gather(own_rows, 'tp', axis=0, tiled=True)  7.28 us
    dot_general x4, matrix products, break_scores(): jnp.einsum('qhd,khd->hqk', query_heads, key_heads, preferred_element_type...  3.93 us
    dot_general x1, matrix products, on_device(): jnp.dot(token_heads, whole_out, preferred_element_type=F32).astype(BF16)  3.01 us
    dynamic_update_slice x4, local copies, waits for them, and re-layouts, absorb_one(): lax.dynamic_update_index_in_dim(inner_pair[1], remain, shard_index, 0)  2.88 us
    another operation x1, loops' own time, on_device(): lax.scan(absorb_one, initial, (jnp.arange(piece_count, dtype=jnp.int32),...  2.84 us
  transfers between devices with their start and end apart: 4, of which 1 were waited for; matrix products, arithmetic and copies ran while one was open for 24% of the time, Pallas kernels for 0%

profile of v1, /device:TPU:25, one launch (start us, length us, event | category | flops | bytes accessed | tf_op | source)
XLA Modules:
  0.0 88.9 jit_solution(10929664528696849787)
XLA Ops:
  6.5 0.0 copy-start
  6.5 0.0 all-gather.2.cloned.1.call-start
  6.6 0.7 all-gather.2.cloned.1.call-update
  7.3 0.1 collective-permute-start
  7.3 1.2 %fusion.25 = f32[128]{0:T(128)S(1)} fusion(bf16[128,2048]{1,0:T(8,128)(2,1)} %param.11), kind=kLoop, calls=%fused_computation.40 | loop fusion | flops 786304 | bytes 524800 | tf_op jit(solution)/shard_map/reduce_sum | solution.py:49
  8.6 0.0 copy-done
  8.6 1.4 %convolution_convert_fusion.3 = bf16[128,256]{1,0:T(8,128)(2,1)S(1)} fusion(bf16[2048,256]{1,0:T(8,128)(2,1)S(1)} %copy-done, bf16[128,2048]{1,0:T(8,128)(2,1)} %param.11, f32[2048]{0:T(1024)} %param.12, f32[128]{0:T(128)S(1)} %add_rsqrt_fusion), kind=kOutput, calls=%fused_computation.37 | convolution fusion | flops 135299072 | bytes 1647104 | tf_op jit(solution)/shard_map/dot_general | solution.py:53
  10.0 0.0 copy-start.2
  10.0 1.8 %convolution_convert_fusion.1 = bf16[128,256]{1,0:T(8,128)(2,1)S(1)} fusion(bf16[2048,256]{1,0:T(8,128)(2,1)} %param.15, bf16[128,2048]{1,0:T(8,128)(2,1)} %param.11, f32[2048]{0:T(1024)} %param.12, f32[128]{0:T(128)S(1)} %add_rsqrt_fusion), kind=kOutput, calls=%fused_computation.35 | convolution fusion | flops 135299072 | bytes 1647104 | tf_op jit(solution)/shard_map/dot_general | solution.py:54
  11.8 0.0 copy-done.1
  11.8 0.0 copy-done.4
  11.8 0.0 copy-done.3
  11.8 0.4 convolution_convert_fusion.2
  12.2 11.1 %all_gather.12 = bf16[512,256]{1,0:T(8,128)(2,1)S(1)} all-gather(bf16[128,256]{1,0:T(8,128)(2,1)S(1)} %convolution_convert_fusion.3), channel_id=1, replica_groups=mesh['grp'=2,'sp'=4,'tp'=4] {'sp'}, dimensions={0}, use_global_device_ids=true | all-gather | bytes 327680 | tf_op jit(solution)/shard_map/all_gather | solution.py:91
  23.3 0.0 collective-permute-done
  23.3 1.5 %collective-permute-start.1 = (bf16[128,4]{0,1:T(4,128)(2,1)S(1)}, bf16[128,4]{0,1:T(4,128)(2,1)S(1)}, u32[]{:S(2)}, u32[]{:S(2)}) collective-permute-start(bf16[128,4]{0,1:T(4,128)(2,1)S(1)} %collective-permute-done), channel_id=1, source_target_pairs={{0,4},{4,8},{8,12},{12,0},{1,5},{5,9},{9,13},{13,1},{2,6},{6,10},{... | collective-permute-start | bytes 3080 | tf_op jit(solution)/shard_map/ppermute | solution.py:97
  24.8 12.3 %all_gather.13 = bf16[512,256]{1,0:T(8,128)(2,1)S(1)} all-gather(bf16[128,256]{1,0:T(8,128)(2,1)S(1)} %convolution_convert_fusion.1), channel_id=1, replica_groups=mesh['grp'=2,'sp'=4,'tp'=4] {'sp'}, dimensions={0}, use_global_device_ids=true | all-gather | bytes 327680 | tf_op jit(solution)/shard_map/all_gather | solution.py:92
  37.1 0.0 collective-permute-done.1
  37.1 0.0 collective-permute-start.2
  37.1 0.2 reshape.91
  37.3 0.3 copy.39
  37.6 0.2 reshape.92
  37.9 0.3 copy.40
  38.1 0.1 copy.37
  38.3 1.7 %collective-permute-done.2 = bf16[128,4]{0,1:T(4,128)(2,1)S(1)} collective-permute-done((bf16[128,4]{0,1:T(4,128)(2,1)S(1)}, bf16[128,4]{0,1:T(4,128)(2,1)S(1)}, u32[]{:S(2)}, u32[]{:S(2)}) %collective-permute-start.2) | collective-permute-done | bytes 1056 | tf_op jit(solution)/shard_map/ppermute | solution.py:97
  40.1 18.4 %while.16 = (s32[]{:T(128)}, f32[4,128,256]{1,2,0:T(8,128)S(1)}, f32[4,4,128]{2,0,1:T(4,128)S(1)}, s32[4]{0:T(128)S(1)}, s32[]{:T(128)}, /*index=5*/s32[]{:T(128...) while((s32[]{:T(128)}, f32[4,128,256]{1,2,0:T(8,128)S(1)}, ...), condition=%wide.region_5.6_spmd.clone, body=%wide.region_1.5_spmd.clone.sunk | while | flops 119505664 | bytes 1446895 | solution.py:115
  40.1 0.6 dynamic_slice.56
  41.4 2.6 %conditional.3 = (f32[1,128,256]{1,2,0:T(8,128)S(1)}, f32[1,4,128]{2,1,0:T(4,128)}) conditional(s32[]{:T(128)} %convert_element_type.82, () %tuple.61, (s32[]{:T(128)}, s32[128]{0:T(128)S(1)}, s32[]{:T(128)}, s32[128]{0:T(128)S(1)}, bf16[4,128,4,64]{1,3,2,0:T(8,128)(2,1)S(1)}, /*index=5*/s32[]{:T(128)}, bf16[128,4,64]{0,2,1:T(8,128)(2,1)S(1)}, ...), branch_computations={%region_2.2_spmd, %region_3.4_spmd} | conditional | flops 119505664 | bytes 1179684 | solution.py:76
  41.4 0.1 broadcast_compare_fusion
  41.5 1.0 %fusion.11 = (f32[4,128]{1,0:T(4,128)}, f32[4,128,128]{1,2,0:T(8,128)S(1)}) fusion(pred[128,128]{0,1:T(8,128)(4,1)S(1)} %broadcast_compare_fusion, f32[4,128]{1,0:T(4,128)S(1)} %convert_bitcast_fusion, bf16[128,4,64]{0,2,1:T(8,128)(2,1)S(1)} %get-tuple-element.246, bf16[4,128,4,64]{1,3,2,0:T(8,128)(2,1)S(1)} %get-tuple-element.244, s32[]{:T(128)} %get-tuple-element.245), kind=kOutput, calls=%fused_computation.14 | convolution fusion | flops 9108992 | bytes 413700 | tf_op jit(solution)/shard_map/while/body/eval_jaxpr/cond/branch_1_fun/qhd,khd->hqk/dot_general | solution.py:15
  42.5 0.7 broadcast_multiply_fusion
  43.2 0.6 fusion.7
  43.8 0.2 fusion.14
  44.0 0.7 dynamic_update_slice.22
  44.7 0.6 dynamic_slice.56
  46.0 2.6 %conditional.3 = (f32[1,128,256]{1,2,0:T(8,128)S(1)}, f32[1,4,128]{2,1,0:T(4,128)}) conditional(s32[]{:T(128)} %convert_element_type.82, () %tuple.61, (s32[]{:T(128)}, s32[128]{0:T(128)S(1)}, s32[]{:T(128)}, s32[128]{0:T(128)S(1)}, bf16[4,128,4,64]{1,3,2,0:T(8,128)(2,1)S(1)}, /*index=5*/s32[]{:T(128)}, bf16[128,4,64]{0,2,1:T(8,128)(2,1)S(1)}, ...), branch_computations={%region_2.2_spmd, %region_3.4_spmd} | conditional | flops 119505664 | bytes 1179684 | solution.py:76
  46.0 0.1 broadcast_compare_fusion
  46.1 1.0 %fusion.11 = (f32[4,128]{1,0:T(4,128)}, f32[4,128,128]{1,2,0:T(8,128)S(1)}) fusion(pred[128,128]{0,1:T(8,128)(4,1)S(1)} %broadcast_compare_fusion, f32[4,128]{1,0:T(4,128)S(1)} %convert_bitcast_fusion, bf16[128,4,64]{0,2,1:T(8,128)(2,1)S(1)} %get-tuple-element.246, bf16[4,128,4,64]{1,3,2,0:T(8,128)(2,1)S(1)} %get-tuple-element.244, s32[]{:T(128)} %get-tuple-element.245), kind=kOutput, calls=%fused_computation.14 | convolution fusion | flops 9108992 | bytes 413700 | tf_op jit(solution)/shard_map/while/body/eval_jaxpr/cond/branch_1_fun/qhd,khd->hqk/dot_general | solution.py:15
  47.1 0.7 broadcast_multiply_fusion
  47.8 0.6 fusion.7
  48.4 0.2 fusion.14
  48.6 0.7 dynamic_update_slice.22
  49.3 0.6 dynamic_slice.56
  50.6 2.6 %conditional.3 = (f32[1,128,256]{1,2,0:T(8,128)S(1)}, f32[1,4,128]{2,1,0:T(4,128)}) conditional(s32[]{:T(128)} %convert_element_type.82, () %tuple.61, (s32[]{:T(128)}, s32[128]{0:T(128)S(1)}, s32[]{:T(128)}, s32[128]{0:T(128)S(1)}, bf16[4,128,4,64]{1,3,2,0:T(8,128)(2,1)S(1)}, /*index=5*/s32[]{:T(128)}, bf16[128,4,64]{0,2,1:T(8,128)(2,1)S(1)}, ...), branch_computations={%region_2.2_spmd, %region_3.4_spmd} | conditional | flops 119505664 | bytes 1179684 | solution.py:76
  50.6 0.1 broadcast_compare_fusion
  50.7 1.0 %fusion.11 = (f32[4,128]{1,0:T(4,128)}, f32[4,128,128]{1,2,0:T(8,128)S(1)}) fusion(pred[128,128]{0,1:T(8,128)(4,1)S(1)} %broadcast_compare_fusion, f32[4,128]{1,0:T(4,128)S(1)} %convert_bitcast_fusion, bf16[128,4,64]{0,2,1:T(8,128)(2,1)S(1)} %get-tuple-element.246, bf16[4,128,4,64]{1,3,2,0:T(8,128)(2,1)S(1)} %get-tuple-element.244, s32[]{:T(128)} %get-tuple-element.245), kind=kOutput, calls=%fused_computation.14 | convolution fusion | flops 9108992 | bytes 413700 | tf_op jit(solution)/shard_map/while/body/eval_jaxpr/cond/branch_1_fun/qhd,khd->hqk/dot_general | solution.py:15
  51.7 0.7 broadcast_multiply_fusion
  52.4 0.6 fusion.7
  53.0 0.2 fusion.14
  53.2 0.7 dynamic_update_slice.22
  53.9 0.6 dynamic_slice.56
  55.2 2.6 %conditional.3 = (f32[1,128,256]{1,2,0:T(8,128)S(1)}, f32[1,4,128]{2,1,0:T(4,128)}) conditional(s32[]{:T(128)} %convert_element_type.82, () %tuple.61, (s32[]{:T(128)}, s32[128]{0:T(128)S(1)}, s32[]{:T(128)}, s32[128]{0:T(128)S(1)}, bf16[4,128,4,64]{1,3,2,0:T(8,128)(2,1)S(1)}, /*index=5*/s32[]{:T(128)}, bf16[128,4,64]{0,2,1:T(8,128)(2,1)S(1)}, ...), branch_computations={%region_2.2_spmd, %region_3.4_spmd} | conditional | flops 119505664 | bytes 1179684 | solution.py:76
  55.2 0.1 broadcast_compare_fusion
  55.3 1.0 %fusion.11 = (f32[4,128]{1,0:T(4,128)}, f32[4,128,128]{1,2,0:T(8,128)S(1)}) fusion(pred[128,128]{0,1:T(8,128)(4,1)S(1)} %broadcast_compare_fusion, f32[4,128]{1,0:T(4,128)S(1)} %convert_bitcast_fusion, bf16[128,4,64]{0,2,1:T(8,128)(2,1)S(1)} %get-tuple-element.246, bf16[4,128,4,64]{1,3,2,0:T(8,128)(2,1)S(1)} %get-tuple-element.244, s32[]{:T(128)} %get-tuple-element.245), kind=kOutput, calls=%fused_computation.14 | convolution fusion | flops 9108992 | bytes 413700 | tf_op jit(solution)/shard_map/while/body/eval_jaxpr/cond/branch_1_fun/qhd,khd->hqk/dot_general | solution.py:15
  56.3 0.7 broadcast_multiply_fusion
  57.0 0.6 fusion.7
  57.6 0.2 fusion.14
  57.8 0.7 dynamic_update_slice.22
  58.5 0.1 fusion.24
  58.7 0.1 copy.43
  58.8 12.2 %all_to_all.16 = bf16[4,32,256]{2,1,0:T(8,128)(2,1)S(1)} all-to-all(bf16[4,32,256]{2,1,0:T(8,128)(2,1)S(1)} %bitcast.57), channel_id=1, replica_groups=mesh['grp'=2,'sp'=4,'tp'=4] {'tp'}, dimensions={0} | all-to-all | bytes 131072 | tf_op jit(solution)/shard_map/all_to_all | solution.py:125
  71.0 3.0 %convolution_convert_fusion = bf16[32,2048]{1,0:T(8,128)(2,1)S(1)} fusion(bf16[32,1024]{1,0:T(8,128)(2,1)S(1)} %bitcast.56, bf16[1024,2048]{1,0:T(8,128)(2,1)} %all-gather.2.cloned.1.call-done), kind=kOutput, calls=%fused_computation.32 | convolution fusion | flops 134283264 | bytes 4390912 | tf_op jit(solution)/shard_map/dot_general | solution.py:127
  74.0 7.3 %all_gather.15 = bf16[128,2048]{1,0:T(8,128)(2,1)S(1)} all-gather(bf16[32,2048]{1,0:T(8,128)(2,1)S(1)} %convolution_convert_fusion), channel_id=1, replica_groups=mesh['grp'=2,'sp'=4,'tp'=4] {'tp'}, dimensions={0}, use_global_device_ids=true | all-gather | bytes 655360 | tf_op jit(solution)/shard_map/all_gather | solution.py:128
  81.3 0.8 copy.80
  (37 shorter events, 0.4 us)
Async XLA Ops:
  6.5 2.0 %copy-start = (bf16[2048,256]{1,0:T(8,128)(2,1)S(1)}, bf16[2048,256]{1,0:T(8,128)(2,1)}, u32[]{:S(2)}) copy-start(bf16[2048,256]{1,0:T(8,128)(2,1)} %param.14) | copy-start | bytes 3145732
  6.5 5.2 %copy-start.1 = (bf16[128,2048]{1,0:T(8,128)(2,1)S(1)}, bf16[128,2048]{1,0:T(8,128)(2,1)}, u32[]{:S(2)}) copy-start(bf16[128,2048]{1,0:T(8,128)(2,1)} %param.11) | copy-start | bytes 1572868
  6.5 5.2 %copy-start.4 = (f32[2048]{0:T(1024)S(1)}, f32[2048]{0:T(1024)}, u32[]{:S(2)}) copy-start(f32[2048]{0:T(1024)} %param.12) | copy-start | bytes 24580
  6.5 5.3 %copy-start.3 = (bf16[2048,256]{1,0:T(8,128)(2,1)S(1)}, bf16[2048,256]{1,0:T(8,128)(2,1)}, u32[]{:S(2)}) copy-start(bf16[2048,256]{1,0:T(8,128)(2,1)} %param.13) | copy-start | bytes 3145732
  6.5 64.5 %all-gather.2.cloned.1.call-start = ((), (), s32[]{:S(2)}) async-start(), calls=%async_computation.1 | async-start | bytes 5242880 | tf_op jit(solution)/shard_map/all_gather | solution.py:126
  7.3 16.0 %collective-permute-start = (bf16[128,4]{0,1:T(4,128)(2,1)}, bf16[128,4]{0,1:T(4,128)(2,1)S(1)}, u32[]{:S(2)}, u32[]{:S(2)}) collective-permute-start(bf16[128,4]{0,1:T(4,128)(2,1)} %bitcast.60), channel_id=1, source_target_pairs={{0,4},{4,8},{8,12},{12,0},{1,5},{5,9},{9,13},{13,1},{2,6},{6,10},{... | collective-permute-start | bytes 3080 | tf_op jit(solution)/shard_map/ppermute | solution.py:97
  10.0 29.9 %copy-start.2 = (bf16[4,128]{1,0:T(4,128)(2,1)S(1)}, bf16[4,128]{1,0:T(4,128)(2,1)}, u32[]{:S(2)}) copy-start(bf16[4,128]{1,0:T(4,128)(2,1)} %param.17) | copy-start | bytes 3076
  23.3 13.8 %collective-permute-start.1 = (bf16[128,4]{0,1:T(4,128)(2,1)S(1)}, bf16[128,4]{0,1:T(4,128)(2,1)S(1)}, u32[]{:S(2)}, u32[]{:S(2)}) collective-permute-start(bf16[128,4]{0,1:T(4,128)(2,1)S(1)} %collective-permute-done), channel_id=1, source_target_pairs={{0,4},{4,8},{8,12},{12,0},{1,5},{5,9},{9,13},{13,1},{2,6},{6,10},{... | collective-permute-start | bytes 3080 | tf_op jit(solution)/shard_map/ppermute | solution.py:97
  37.1 2.8 %collective-permute-start.2 = (bf16[128,4]{0,1:T(4,128)(2,1)S(1)}, bf16[128,4]{0,1:T(4,128)(2,1)S(1)}, u32[]{:S(2)}, u32[]{:S(2)}) collective-permute-start(bf16[128,4]{0,1:T(4,128)(2,1)S(1)} %collective-permute-done.1), channel_id=1, source_target_pairs={{0,4},{4,8},{8,12},{12,0},{1,5},{5,9},{9,13},{13,1},{2,6},{6,10},{... | collective-permute-start | bytes 3080 | tf_op jit(solution)/shard_map/ppermute | solution.py:97
Sparse Core Ops, SparseCore 0:
  8.9 35.8 all-gather.1
